TPU v7x, 256 devices: a whole 4x4x8 slice. The times are simulated.
256 devices in a mesh: sp: 32 (over z, x), tp: 8 (over y, core).
Axes of the slice: x: 4, y: 4, z: 8, core: 2. Of those that a mesh axis runs over, the one named last changes fastest.
Arguments:
- tokens: bfloat16 [8192, 4096], P('sp', 'tp'), may hold values from -6 to 6
- pre_gain: float32 [4096], replicated, may hold values from 0.1 to 1.9
- rate_factor: float32 [8192], P('sp'), may hold values from 0.5 to 2, as said below
- w_rec_in: bfloat16 [4096, 1024], P(None, 'tp'), may hold values from -0.09375 to 0.09375
- w_rec_gate: bfloat16 [4096, 1024], P(None, 'tp')
- conv_taps: float32 [4, 1024], P(None, 'tp'), may hold values from -3 to 3
- rate_maps: bfloat16 [8, 128, 128], P('tp'), may hold values from -0.5 to 0.5
- input_maps: bfloat16 [8, 128, 128], P('tp'), may hold values from -0.5 to 0.5
- decay_param: float32 [1024], P('tp'), as said below
- w_query: bfloat16 [4096, 1536], P(None, 'tp'), may hold values from -0.09375 to 0.09375
- w_latent: bfloat16 [4096, 512], replicated, may hold values from -0.09375 to 0.09375
- w_rope_key: bfloat16 [4096, 64], replicated, may hold values from -0.09375 to 0.09375
- latent_gain: float32 [512], replicated, may hold values from 0.7 to 100, as said below
- w_expand: bfloat16 [512, 2048], P(None, 'tp')
- rec_gain: float32 [1024], P('tp'), may hold values from 0.1 to 1.9
- att_gain: float32 [1024], P('tp'), may hold values from 0.1 to 1.9
- w_out_rec: bfloat16 [1024, 4096], P('tp'), may hold values from -0.125 to 0.125
- w_out_att: bfloat16 [1024, 4096], P('tp'), may hold values from -0.125 to 0.125
- post_gain: float32 [4096], replicated, may hold values from 0.1 to 1.9
Outputs:
- layer_out: bfloat16 [8192, 4096], P(('sp', 'tp'))
Inputs may be any that keep to these rules, and one draw needn't show every extreme that they name: `rate_factor`: one positive factor for each position. `decay_param`: one parameter for each recurrent channel. `latent_gain`: one positive gain for each latent entry.
All inputs are finite; a program needn't handle non-finite values.
Results may differ from a plain program's by a relative error of at most 0.017.
The roundings to bfloat16 on the way count: a program that leaves them out, or rounds other values in their place, can miss the bound.
Values may be sent and summed in bfloat16 or wider, within the bound.
A program may use at most 128 MiB of HBM per device.

v0:
```python
import math
import jax
import jax.numpy as jnp
from jax import lax
from jax.sharding import PartitionSpec as P

NOPE = 128
ROPE = 64
VDIM = 128
EPS = 1e-06
RATE_C = 8.0
THETA = 10000.0
span_limit = 2048


def passed_along(block, axis, distance):
    devices = range(lax.axis_size(axis))
    route = [(i - distance, i) for i in devices if i - distance in devices]
    return lax.ppermute(block, axis, route)


def from_everyone(shard, axis):
    copies = jnp.broadcast_to(shard, (lax.axis_size(axis), *shard.shape))
    return lax.all_to_all(copies, axis, split_axis=0, concat_axis=0, tiled=True)


def all_in_one(shard, axis):
    leaves = jax.tree.leaves(shard)
    order = sorted(range(len(leaves)), key=lambda k: -leaves[k].size)
    width = (1, *leaves[order[0]].shape)[-1]
    lines = [
        jnp.pad(leaves[k].reshape(-1), (0, -leaves[k].size % width)).reshape(-1, width)
        for k in order
    ]
    both, at, found = (from_everyone(jnp.concatenate(lines), axis), 0, {})
    for k, line in zip(order, lines):
        slab = both[:, at : at + len(line)].reshape(len(both), -1)
        found[k] = slab[:, : leaves[k].size].reshape(-1, *leaves[k].shape)
        at += len(line)
    numbers = iter(range(len(leaves)))
    return jax.tree.map(lambda _: found[next(numbers)], shard)


def joined_by_halves(pieces, combine):
    while len(jax.tree.leaves(pieces)[0]) > 1:
        pieces = jax.vmap(combine)(
            *(jax.tree.map(lambda part: part[side::2], pieces) for side in (0, 1))
        )
    return jax.tree.map(lambda part: part[0], pieces)


def entering(shard, axis, combine, identity):
    count, mine = (lax.axis_size(axis), lax.axis_index(axis))
    passed = jnp.arange(count) < mine

    def kept(part, zero, own):
        part = jnp.where(
            passed.reshape(-1, *(1 for _ in own.shape)), part, jnp.asarray(zero, own.dtype)
        )
        return part

    pieces = all_in_one(shard, axis)
    return joined_by_halves(jax.tree.map(kept, pieces, identity, shard), combine)


def of_everyone(shard, axis):
    return from_everyone(shard, axis).sum(axis=0)


def in_one_piece(arrays, axis, dim, along):
    widths = [a.shape[along] for a in arrays]
    both = jnp.concatenate(arrays, axis=along)
    out = lax.all_gather(both, axis, axis=dim, tiled=True)
    return tuple(jnp.split(out, [sum(widths[:k]) for k in range(1, len(widths))], axis=along))


def in_blocks(shard, dim, count):
    before, after = (shard.shape[:dim], shard.shape[dim + 1 :])
    return jnp.moveaxis(shard.reshape(*before, count, -1, *after), dim, 0)


def sum_at_owner(shard, axis, dim):
    count = lax.axis_size(axis)
    pieces = lax.all_to_all(in_blocks(shard, dim, count), axis, 0, 0, tiled=True)
    return jnp.sum(pieces.astype(jnp.float32), axis=0)


def rms_inverse(values):
    return lax.rsqrt(jnp.mean(values * values, axis=-1, keepdims=True) + EPS)


def rotate(values, cosine, sine_part):
    half_width = values.shape[-1] // 2
    leading = values[..., :half_width]
    trailing = values[..., half_width:]
    return jnp.concatenate(
        [leading * cosine - trailing * sine_part, trailing * cosine + leading * sine_part], axis=-1
    )


def angles(length, offset, span_width):
    frequency = 1.0 / THETA ** (jnp.arange(0, span_width, 2).astype(jnp.float32) / span_width)
    places = (offset + jnp.arange(length)).astype(jnp.float32)
    turned = places[:, None] * frequency[None, :]
    return (jnp.cos(turned), jnp.sin(turned))


def combine_steps(earlier, later):
    return (earlier[0] * later[0], later[0] * earlier[1] + later[1])


def attend_block(state_now, query_nope, query_rope, places, keys_nope, key_rope, values, key_root):
    maxima, totals, accumulated = state_now
    scaling = 1.0 / math.sqrt(query_nope.shape[-1] + query_rope.shape[-1])
    scores = jnp.einsum("qhd,khd->hqk", query_nope, keys_nope, preferred_element_type=jnp.float32)
    scores = scores + jnp.einsum(
        "qhd,kd->hqk", query_rope, key_rope, preferred_element_type=jnp.float32
    )
    scores = scores * scaling
    key_places = key_root + jnp.arange(keys_nope.shape[0])
    visible = key_places[None, :] <= places[:, None]
    scores = jnp.where(visible[None], scores, -jnp.inf)
    largest = jnp.maximum(maxima, jnp.max(scores, axis=-1))
    anchor = jnp.where(largest == -jnp.inf, 0.0, largest)
    weights = jnp.exp(scores - anchor[..., None])
    shrink = jnp.exp(maxima - anchor)
    totals = totals * shrink + jnp.sum(weights, axis=-1)
    accumulated = accumulated * shrink[..., None] + jnp.einsum(
        "hqk,khd->hqd", weights.astype(jnp.bfloat16), values, preferred_element_type=jnp.float32
    )
    return (largest, totals, accumulated)


def shards(
    tokens,
    pre_gain,
    rate_factor,
    w_rec_in,
    w_rec_gate,
    conv_taps,
    rate_maps,
    input_maps,
    decay_param,
    w_query,
    w_latent,
    w_rope_key,
    latent_gain,
    w_expand,
    rec_gain,
    att_gain,
    w_out_rec,
    w_out_att,
    post_gain,
):
    row_count = tokens.shape[0]
    model_width = w_rec_in.shape[0]
    channels = w_rec_in.shape[1]
    heads_here = w_query.shape[1] // (NOPE + ROPE)
    group_size = lax.axis_size("tp")
    first_place = lax.axis_index("sp") * row_count
    places = first_place + jnp.arange(row_count)
    last_place = first_place + row_count - 1
    piece_wide = lax.all_gather(tokens, "tp", axis=1, tiled=True).astype(jnp.float32)
    piece_low = (piece_wide * pre_gain).astype(jnp.bfloat16)

    def accumulate(source, weight):
        return jnp.dot(source, weight, preferred_element_type=jnp.float32)

    squares = jnp.sum(piece_wide * piece_wide, axis=1, keepdims=True)
    sum_input = accumulate(piece_low, w_rec_in)
    sum_gate = accumulate(piece_low, w_rec_gate)
    sum_query = accumulate(piece_low, w_query)
    sum_latent = accumulate(piece_low, w_latent)
    sum_rope = accumulate(piece_low, w_rope_key)
    inverse = lax.rsqrt(squares / model_width + EPS)
    rec_input = (inverse * sum_input).astype(jnp.bfloat16)
    gate_value = inverse * sum_gate
    query_raw = inverse * sum_query
    latent_raw = inverse * sum_latent
    rope_raw = inverse * sum_rope
    taps = conv_taps.shape[0]
    tail_rows = rec_input[row_count - (taps - 1) :]
    before = passed_along(tail_rows, "sp", 1)
    padded = jnp.concatenate([before, rec_input], axis=0)
    convolved = conv_taps[0] * padded[0:row_count].astype(jnp.float32)
    for tap_index in range(1, taps):
        convolved = convolved + conv_taps[tap_index] * padded[
            tap_index : tap_index + row_count
        ].astype(jnp.float32)
    conv_low = convolved.astype(jnp.bfloat16)
    blocks = conv_low.reshape(row_count, rate_maps.shape[0], rate_maps.shape[1])
    rate_gate = jax.nn.sigmoid(
        jnp.einsum("sbi,bij->sbj", blocks, rate_maps, preferred_element_type=jnp.float32)
    ).reshape(row_count, channels)
    entry_gate = jax.nn.sigmoid(
        jnp.einsum("sbi,bij->sbj", blocks, input_maps, preferred_element_type=jnp.float32)
    ).reshape(row_count, channels)
    log_keep = -RATE_C * rate_factor[:, None] * rate_gate * jax.nn.softplus(-decay_param)
    keep_rate = jnp.exp(log_keep)
    driven = jnp.sqrt(-jnp.expm1(2.0 * log_keep)) * entry_gate * convolved
    cum_keep, local_state = lax.associative_scan(combine_steps, (keep_rate, driven), axis=0)
    identity = (jnp.ones((channels,), jnp.float32), jnp.zeros((channels,), jnp.float32))
    chain_keep, carried = entering(
        (cum_keep[row_count - 1], local_state[row_count - 1]), "sp", combine_steps, identity
    )
    state_seq = local_state + cum_keep * carried[None, :]
    rec_out = state_seq * jax.nn.gelu(gate_value)
    rec_squares = jnp.sum(rec_out * rec_out, axis=1, keepdims=True)
    rec_total = of_everyone(rec_squares, "tp")
    cosine, sine_part = angles(row_count, first_place, ROPE)
    query_heads = query_raw.reshape(row_count, heads_here, NOPE + ROPE)
    query_nope = query_heads[:, :, :NOPE].astype(jnp.bfloat16)
    query_rope = rotate(query_heads[:, :, NOPE:], cosine[:, None, :], sine_part[:, None, :]).astype(
        jnp.bfloat16
    )
    own_latent = (latent_raw * rms_inverse(latent_raw) * latent_gain).astype(jnp.bfloat16)
    rope_key = rotate(rope_raw, cosine, sine_part).astype(jnp.bfloat16)
    start_state = (
        jnp.full((heads_here, row_count), -jnp.inf, jnp.float32),
        jnp.zeros((heads_here, row_count), jnp.float32),
        jnp.zeros((heads_here, row_count, VDIM), jnp.float32),
    )
    expanded_local = jnp.dot(own_latent, w_expand, preferred_element_type=jnp.float32).astype(
        jnp.bfloat16
    )
    key_source, rope_source = in_one_piece((expanded_local, rope_key), "sp", 0, 1)
    total_rows = key_source.shape[0]
    key_span = math.gcd(total_rows, span_limit)

    def one_span(span_index, state_inner):
        key_root = span_index * key_span

        def compute(state_deep):
            source_rows = lax.dynamic_slice_in_dim(key_source, span_index * key_span, key_span, 0)
            rope_rows = lax.dynamic_slice_in_dim(rope_source, span_index * key_span, key_span, 0)
            expanded = source_rows
            expanded = expanded.reshape(key_span, heads_here, NOPE + VDIM)
            return attend_block(
                state_deep,
                query_nope,
                query_rope,
                places,
                expanded[:, :, :NOPE],
                rope_rows,
                expanded[:, :, NOPE:],
                key_root,
            )

        def keep_state(state_deep):
            return state_deep

        return lax.cond(key_root <= last_place, compute, keep_state, state_inner)

    maxima, totals, accumulated = lax.fori_loop(0, total_rows // key_span, one_span, start_state)
    att_out = (
        (accumulated / totals[..., None]).transpose(1, 0, 2).reshape(row_count, heads_here * VDIM)
    )
    att_squares = jnp.sum(att_out * att_out, axis=1, keepdims=True)
    att_total = of_everyone(att_squares, "tp")
    rec_norm = (rec_out * lax.rsqrt(rec_total / (channels * group_size) + EPS) * rec_gain).astype(
        jnp.bfloat16
    )
    att_norm = (
        att_out * lax.rsqrt(att_total / (heads_here * VDIM * group_size) + EPS) * att_gain
    ).astype(jnp.bfloat16)
    mixed_sum = sum_at_owner(
        (
            jnp.dot(rec_norm, w_out_rec, preferred_element_type=jnp.float32)
            + jnp.dot(att_norm, w_out_att, preferred_element_type=jnp.float32)
        ).astype(jnp.bfloat16),
        "tp",
        0,
    )
    return (mixed_sum * rms_inverse(mixed_sum) * post_gain).astype(jnp.bfloat16)


def solution(mesh):
    placed = (
        P("sp", "tp"),
        P(),
        P("sp"),
        P(None, "tp"),
        P(None, "tp"),
        P(None, "tp"),
        P("tp", None, None),
        P("tp", None, None),
        P("tp"),
        P(None, "tp"),
        P(),
        P(),
        P(),
        P(None, "tp"),
        P("tp"),
        P("tp"),
        P("tp", None),
        P("tp", None),
        P(),
    )
    return jax.shard_map(
        shards, mesh=mesh, in_specs=placed, out_specs=P(("sp", "tp"), None), check_vma=False
    )
```

profile of v0, /device:TPU:228, one launch (start us, length us, event | category | flops | bytes accessed | tf_op | source)
XLA Modules:
  0.0 218.6 jit_solution(17442014184566971345)
XLA Ops:
  7.3 30.1 %all-gather.3.cloned.1.call-done = bf16[256,4096]{1,0:T(8,128)(2,1)} async-done(((bf16[256,512]{1,0:T(8,128)(2,1)}), bf16[256,4096]{1,0:T(8,128)(2,1)}) %all-gather.3.cloned.1.call-update) | async-done | bytes 2097168 | tf_op jit(solution)/shard_map/all_gather | solution.py:163
  37.5 2.2 %fusion.16 = f32[256]{0:T(256)S(1)} fusion(bf16[256,4096]{1,0:T(8,128)(2,1)} %all-gather.3.cloned.1.call-done), kind=kLoop, calls=%fused_computation.29 | loop fusion | flops 3145472 | bytes 2098176 | tf_op jit(solution)/shard_map/reduce_sum | solution.py:169
  39.7 3.6 %multiply_reduce_fusion.1 = (f32[256]{0:T(256)S(1)}, f32[256,512]{1,0:T(8,128)S(1)}) fusion(bf16[4096,512]{1,0:T(8,128)(2,1)} %param.33, bf16[256,4096]{1,0:T(8,128)(2,1)S(1)} %copy-done.1, f32[4096]{0:T(1024)S(1)} %copy-done.14, f32[256]{0:T(256)S(1)} %add_rsqrt_fusion.3), kind=kOutput, calls=%fused_computation.55 | convolution fusion | flops 1077280512 | bytes 6834176 | tf_op jit(solution)/shard_map/dot_general | solution.py:167
  45.6 2.7 %fusion.29 = bf16[256,128]{1,0:T(8,128)(2,1)S(1)} fusion(bf16[4096,128]{1,0:T(8,128)(2,1)} %param.26, bf16[256,4096]{1,0:T(8,128)(2,1)} %all-gather.3.cloned.1.call-done, f32[4096]{0:T(1024)S(1)} %copy-done.14, f32[256]{0:T(256)S(1)} %add_rsqrt_fusion.3), kind=kOutput, calls=%fused_computation.50 | convolution fusion | flops 271646720 | bytes 3228672 | tf_op jit(solution)/shard_map/dot_general | solution.py:167
  48.3 3.1 %collective-permute-start = (bf16[3,128]{1,0:T(4,128)(2,1)S(1)}, bf16[3,128]{1,0:T(4,128)(2,1)S(1)}, u32[]{:S(2)}, u32[]{:S(2)}) collective-permute-start(bf16[3,128]{1,0:T(4,128)(2,1)S(1)} %slice.463), channel_id=1, source_target_pairs={{0,8},{8,16},{16,24},{24,32},{32,40},{40,48},{48,56},{56,64},{64,7... | collective-permute-start | bytes 2312 | tf_op jit(solution)/shard_map/ppermute | solution.py:19
  52.3 1.4 collective-permute-done
  56.8 10.5 %all-to-all-start = ((f32[32,2,128]{2,1,0:T(2,128)}), f32[32,2,128]{2,1,0:T(2,128)S(1)}, u32[]{:S(2)}, u32[]{:S(2)}) async-start(f32[32,2,128]{2,1,0:T(2,128)} %broadcast_in_dim.42), calls=%async_computation | async-start | bytes 65536 | tf_op jit(solution)/shard_map/all_to_all | solution.py:24
  67.5 5.4 %all-to-all-done = f32[32,2,128]{2,1,0:T(2,128)S(1)} async-done(((f32[32,2,128]{2,1,0:T(2,128)}), f32[32,2,128]{2,1,0:T(2,128)S(1)}, u32[]{:S(2)}, u32[]{:S(2)}) %all-to-all-start) | async-done | bytes 32800 | tf_op jit(solution)/shard_map/all_to_all | solution.py:24
  73.3 2.7 %multiply_reduce_fusion.2 = (f32[256]{0:T(256)S(1)}, f32[256,128]{1,0:T(8,128)S(1)}) fusion(bf16[4096,128]{1,0:T(8,128)(2,1)} %param.27, bf16[256,4096]{1,0:T(8,128)(2,1)} %all-gather.3.cloned.1.call-done, f32[4096]{0:T(1024)S(1)} %copy-done.14, f32[256]{0:T(256)S(1)} %add_rsqrt_fusion.3, f32[128]{0:T(128)S(1)} %add_bitcast_fusion, ...), kind=kOutput, calls=%fused_computation.75 | convolution fusion | flops 272105216 | bytes 3820032 | tf_op jit(solution)/shard_map/dot_general | solution.py:167
  76.6 3.4 %all-to-all-start.1 = ((f32[8,256,1]{1,2,0:T(1,128)}), f32[8,256,1]{1,2,0:T(1,128)S(1)}, u32[]{:S(2)}, u32[]{:S(2)}) async-start(f32[8,256,1]{1,2,0:T(1,128)} %broadcast_in_dim.45), calls=%async_computation.1 | async-start | bytes 16384 | tf_op jit(solution)/shard_map/all_to_all | solution.py:24
  80.2 5.2 %all-to-all-done.1 = f32[8,256,1]{1,2,0:T(1,128)S(1)} async-done(((f32[8,256,1]{1,2,0:T(1,128)}), f32[8,256,1]{1,2,0:T(1,128)S(1)}, u32[]{:S(2)}, u32[]{:S(2)}) %all-to-all-start.1) | async-done | bytes 8224 | tf_op jit(solution)/shard_map/all_to_all | solution.py:24
  85.4 49.2 %all-gather.5.cloned.1.call-done = bf16[8192,320]{0,1:T(8,128)(2,1)} async-done(((bf16[256,320]{0,1:T(8,128)(2,1)}), bf16[8192,320]{0,1:T(8,128)(2,1)}) %all-gather.5.cloned.1.call-update) | async-done | bytes 5242896 | tf_op jit(solution)/shard_map/all_gather | solution.py:73
  134.6 4.7 %split.8 = bf16[8192,256]{0,1:T(8,128)(2,1)} slice(bf16[8192,320]{0,1:T(8,128)(2,1)} %all-gather.5.cloned.1.call-done), slice={[0:8192], [0:256]} | slice | bytes 8388608 | tf_op jit(solution)/shard_map/split | solution.py:74
  139.3 6.4 %copy.31 = bf16[8192,256]{1,0:T(8,128)(2,1)} copy(bf16[8192,256]{0,1:T(8,128)(2,1)} %split.8) | data formatting | bytes 8388608
  146.9 1.8 copy.33
  148.7 17.6 %while.18 = (s32[]{:T(128)}, f32[1,256]{1,0:T(1,128)S(1)}, f32[1,256]{1,0:T(1,128)S(1)}, f32[1,256,128]{2,1,0:T(8,128)S(1)}, s32[]{:T(128)}, /*index=5*/bf16[819...) while((s32[]{:T(128)}, f32[1,256]{1,0:T(1,128)S(1)}, ...), condition=%wide.region_9.10_spmd.clone, body=%wide.region_4.9_spmd.clone.sunk | while | flops 340332288 | bytes 14554469 | solution.py:254
  148.7 4.4 %conditional.3 = ((f32[1,256]{1,0:T(1,128)S(1)}, f32[1,256]{1,0:T(1,128)S(1)}, f32[1,256,128]{2,1,0:T(8,128)S(1)})) conditional(s32[]{:T(128)} %convert_element_type.205, (f32[1,256]{1,0:T(1,128)S(1)}, f32[1,256]{1,0:T(1,128)S(1)}, f32[1,256,128]{2,1,0:T(8,128)S(1)}) %tuple.82, (s32[]{:T(128)}, s32[]{:T(128)}, s32[]{:T(128)}, ...), branch_computations={%region_5.5_spmd, %region_6.8_spmd} | conditional | flops 340332288 | bytes 14553182 | solution.py:252
  148.8 1.3 dynamic-slice_bitcast_fusion
  150.1 1.5 convolution_bitcast_fusion
  153.1 4.3 %conditional.3 = ((f32[1,256]{1,0:T(1,128)S(1)}, f32[1,256]{1,0:T(1,128)S(1)}, f32[1,256,128]{2,1,0:T(8,128)S(1)})) conditional(s32[]{:T(128)} %convert_element_type.205, (f32[1,256]{1,0:T(1,128)S(1)}, f32[1,256]{1,0:T(1,128)S(1)}, f32[1,256,128]{2,1,0:T(8,128)S(1)}) %tuple.82, (s32[]{:T(128)}, s32[]{:T(128)}, s32[]{:T(128)}, ...), branch_computations={%region_5.5_spmd, %region_6.8_spmd} | conditional | flops 340332288 | bytes 14553182 | solution.py:252
  153.2 1.3 dynamic-slice_bitcast_fusion
  154.5 1.4 convolution_bitcast_fusion
  157.5 4.4 %conditional.3 = ((f32[1,256]{1,0:T(1,128)S(1)}, f32[1,256]{1,0:T(1,128)S(1)}, f32[1,256,128]{2,1,0:T(8,128)S(1)})) conditional(s32[]{:T(128)} %convert_element_type.205, (f32[1,256]{1,0:T(1,128)S(1)}, f32[1,256]{1,0:T(1,128)S(1)}, f32[1,256,128]{2,1,0:T(8,128)S(1)}) %tuple.82, (s32[]{:T(128)}, s32[]{:T(128)}, s32[]{:T(128)}, ...), branch_computations={%region_5.5_spmd, %region_6.8_spmd} | conditional | flops 340332288 | bytes 14553182 | solution.py:252
  157.6 1.3 dynamic-slice_bitcast_fusion
  158.9 1.5 convolution_bitcast_fusion
  161.9 4.3 %conditional.3 = ((f32[1,256]{1,0:T(1,128)S(1)}, f32[1,256]{1,0:T(1,128)S(1)}, f32[1,256,128]{2,1,0:T(8,128)S(1)})) conditional(s32[]{:T(128)} %convert_element_type.205, (f32[1,256]{1,0:T(1,128)S(1)}, f32[1,256]{1,0:T(1,128)S(1)}, f32[1,256,128]{2,1,0:T(8,128)S(1)}) %tuple.82, (s32[]{:T(128)}, s32[]{:T(128)}, s32[]{:T(128)}, ...), branch_computations={%region_5.5_spmd, %region_6.8_spmd} | conditional | flops 340332288 | bytes 14553182 | solution.py:252
  162.0 1.3 dynamic-slice_bitcast_fusion
  163.3 1.4 convolution_bitcast_fusion
  167.1 4.3 %all-to-all-start.2 = ((f32[8,256,1]{1,2,0:T(1,128)}), f32[8,256,1]{1,2,0:T(1,128)S(1)}, u32[]{:S(2)}, u32[]{:S(2)}) async-start(f32[8,256,1]{1,2,0:T(1,128)} %broadcast_in_dim.72), calls=%async_computation.2 | async-start | bytes 16384 | tf_op jit(solution)/shard_map/all_to_all | solution.py:24
  171.4 4.0 %fusion.54 = f32[256,4096]{1,0:T(8,128)} fusion(bf16[128,4096]{1,0:T(8,128)(2,1)} %param.39, f32[256,128]{1,0:T(8,128)S(1)} %get-tuple-element.364, f32[128]{0:T(128)S(1)} %copy-done.7, f32[256]{0:T(256)S(1)} %add_rsqrt_fusion.2), kind=kOutput, calls=%fused_computation.81 | convolution fusion | flops 268533760 | bytes 5375488 | tf_op jit(solution)/shard_map/dot_general | solution.py:268
  176.7 3.0 %fusion.15 = bf16[256,4096]{1,0:T(8,128)(2,1)S(1)} fusion(f32[256,4096]{1,0:T(8,128)} %fusion.54, bf16[128,4096]{1,0:T(8,128)(2,1)S(1)} %copy-done.3, f32[128]{0:T(128)S(1)} %copy-done.10, f32[256]{0:T(256)S(1)} %add_rsqrt_fusion, f32[1,256,128]{2,1,0:T(8,128)S(1)} %get-tuple-element.220, f32[256]{0:T(256)S(1)} %bitcast.96), kind=kOutput, calls=%fused_computation.28 | convolution fusion | flops 270663680 | bytes 7473664 | tf_op jit(solution)/shard_map/dot_general | solution.py:269
  179.7 30.5 %all_to_all.20 = bf16[8,32,4096]{2,1,0:T(8,128)(2,1)S(1)} all-to-all(bf16[8,32,4096]{2,1,0:T(8,128)(2,1)S(1)} %bitcast.87), channel_id=1, replica_groups=mesh['sp'=32,'tp'=8] {'tp'}, dimensions={0} | all-to-all | bytes 4194304 | tf_op jit(solution)/shard_map/all_to_all | solution.py:84
  (258 shorter events, 18.6 us)
Async XLA Ops:
  6.5 44.8 %copy-start = (bf16[4096,192]{0,1:T(8,128)(2,1)S(1)}, bf16[4096,192]{0,1:T(8,128)(2,1)}, u32[]{:S(2)}) copy-start(bf16[4096,192]{0,1:T(8,128)(2,1)} %param.32) | copy-start | bytes 4718596
  6.5 33.2 %copy-start.14 = (f32[4096]{0:T(1024)S(1)}, f32[4096]{0:T(1024)}, u32[]{:S(2)}) copy-start(f32[4096]{0:T(1024)} %param.24) | copy-start | bytes 49156
  6.5 30.9 %all-gather.3.cloned.1.call-start = ((), (), s32[]{:S(2)}) async-start(), calls=%async_computation.4 | async-start | bytes 2359296 | tf_op jit(solution)/shard_map/all_gather | solution.py:163
  7.3 127.3 %all-gather.5.cloned.1.call-start = ((), (), s32[]{:S(2)}) async-start(), calls=%async_computation.5 | async-start | bytes 5406720 | tf_op jit(solution)/shard_map/all_gather | solution.py:73
  37.5 2.3 %copy-start.1 = (bf16[256,4096]{1,0:T(8,128)(2,1)S(1)}, bf16[256,4096]{1,0:T(8,128)(2,1)}, u32[]{:S(2)}) copy-start(bf16[256,4096]{1,0:T(8,128)(2,1)} %all-gather.3.cloned.1.call-done) | copy-start | bytes 6291460
  39.7 3.6 %copy-start.11 = (bf16[4096,64]{0,1:T(8,128)(2,1)S(1)}, bf16[4096,64]{0,1:T(8,128)(2,1)}, u32[]{:S(2)}) copy-start(bf16[4096,64]{0,1:T(8,128)(2,1)} %param.34) | copy-start | bytes 1572868
  43.3 1.1 copy-start.4
  43.3 1.1 copy-start.6
  43.4 2.1 copy-start.15
  43.4 2.1 copy-start.9
  43.4 2.1 copy-start.8
  45.5 5.9 %copy-start.2 = (bf16[256,4096]{1,0:T(8,128)(2,1)S(1)}, bf16[256,4096]{1,0:T(8,128)(2,1)}, u32[]{:S(2)}) copy-start(bf16[256,4096]{1,0:T(8,128)(2,1)} %all-gather.3.cloned.1.call-done) | copy-start | bytes 6291460
  48.3 5.5 %copy-start.12 = (bf16[1,128,128]{2,1,0:T(8,128)(2,1)S(1)}, bf16[1,128,128]{2,1,0:T(8,128)(2,1)}, u32[]{:S(2)}) copy-start(bf16[1,128,128]{2,1,0:T(8,128)(2,1)} %param.29) | copy-start | bytes 98308
  48.3 5.7 %copy-start.13 = (bf16[1,128,128]{2,1,0:T(8,128)(2,1)S(1)}, bf16[1,128,128]{2,1,0:T(8,128)(2,1)}, u32[]{:S(2)}) copy-start(bf16[1,128,128]{2,1,0:T(8,128)(2,1)} %param.30) | copy-start | bytes 98308
  48.3 5.5 %collective-permute-start = (bf16[3,128]{1,0:T(4,128)(2,1)S(1)}, bf16[3,128]{1,0:T(4,128)(2,1)S(1)}, u32[]{:S(2)}, u32[]{:S(2)}) collective-permute-start(bf16[3,128]{1,0:T(4,128)(2,1)S(1)} %slice.463), channel_id=1, source_target_pairs={{0,8},{8,16},{16,24},{24,32},{32,40},{40,48},{48,56},{56,64},{64,7... | collective-permute-start | bytes 2312 | tf_op jit(solution)/shard_map/ppermute | solution.py:19
  56.8 16.1 %all-to-all-start = ((f32[32,2,128]{2,1,0:T(2,128)}), f32[32,2,128]{2,1,0:T(2,128)S(1)}, u32[]{:S(2)}, u32[]{:S(2)}) async-start(f32[32,2,128]{2,1,0:T(2,128)} %broadcast_in_dim.42), calls=%async_computation | async-start | bytes 65536 | tf_op jit(solution)/shard_map/all_to_all | solution.py:24
  76.6 8.7 %all-to-all-start.1 = ((f32[8,256,1]{1,2,0:T(1,128)}), f32[8,256,1]{1,2,0:T(1,128)S(1)}, u32[]{:S(2)}, u32[]{:S(2)}) async-start(f32[8,256,1]{1,2,0:T(1,128)} %broadcast_in_dim.45), calls=%async_computation.1 | async-start | bytes 16384 | tf_op jit(solution)/shard_map/all_to_all | solution.py:24
  145.7 1.2 slice-start
  148.7 22.7 %copy-start.7 = (f32[128]{0:T(128)S(1)}, f32[128]{0:T(128)}, u32[]{:S(2)}) copy-start(f32[128]{0:T(128)} %param.37) | copy-start | bytes 1540
  167.1 9.6 %all-to-all-start.2 = ((f32[8,256,1]{1,2,0:T(1,128)}), f32[8,256,1]{1,2,0:T(1,128)S(1)}, u32[]{:S(2)}, u32[]{:S(2)}) async-start(f32[8,256,1]{1,2,0:T(1,128)} %broadcast_in_dim.72), calls=%async_computation.2 | async-start | bytes 16384 | tf_op jit(solution)/shard_map/all_to_all | solution.py:24
  171.4 5.3 %copy-start.3 = (bf16[128,4096]{1,0:T(8,128)(2,1)S(1)}, bf16[128,4096]{1,0:T(8,128)(2,1)}, u32[]{:S(2)}) copy-start(bf16[128,4096]{1,0:T(8,128)(2,1)} %param.40) | copy-start | bytes 3145732
  171.4 5.3 %copy-start.10 = (f32[128]{0:T(128)S(1)}, f32[128]{0:T(128)}, u32[]{:S(2)}) copy-start(f32[128]{0:T(128)} %param.38) | copy-start | bytes 1540
  210.2 0.7 copy-start.5
Sparse Core Ops, SparseCore 0:
  9.2 28.2 all-gather.2
  45.6 88.9 all-gather.4
where the time goes:
time: 220 us; the launch traced here: 219 us
  waiting for transfers between devices  93.3 us (42%)
  blocking collectives  30.5 us (14%)
  matrix products  28.8 us (13%)
  local copies, waits for them, and re-layouts  22.8 us (10%)
  starting transfers between devices  21.3 us (10%)
  between operations  14.5 us (7%)
  other arithmetic  6.97 us (3%)
    all_gather x1, waiting for transfers between devices, in_one_piece(): out = lax.all_gather(both, axis, axis=dim, tiled=True)  49.2 us
    all_to_all x1, blocking collectives, sum_at_owner(): lax.all_to_all(in_blocks(shard, dim, count), axis, 0, 0, tiled=True)  30.5 us
    all_gather x1, waiting for transfers between devices, shards(): lax.all_gather(tokens, 'tp', axis=1, tiled=True).astype(jnp.float32)  30.1 us
    all_to_all x3, starting transfers between devices, from_everyone(): return lax.all_to_all(copies, axis, split_axis=0, concat_axis=0, tiled=True)  18.2 us
    all_to_all x3, waiting for transfers between devices, from_everyone(): return lax.all_to_all(copies, axis, split_axis=0, concat_axis=0, tiled=True)  11.9 us
    dot_general x5, matrix products, accumulate(): return jnp.dot(source, weight, preferred_element_type=jnp.float32)  10.7 us
    unnamed x35, local copies, waits for them, and re-layouts  8.57 us
    split x3, local copies, waits for them, and re-layouts, in_one_piece(): jnp.split(out, [sum(widths[:k]) for k in range(1, len(widths))], axis=along)  5.93 us
  transfers between devices with their start and end apart: 6, of which 6 were waited for; matrix products, arithmetic and copies ran while one was open for 6% of the time, Pallas kernels for 0%

commit v1 on v0

--- a/solution.py
+++ b/solution.py
@@ -11,6 +11,33 @@
 RATE_C = 8.0
 THETA = 10000.0
 span_limit = 2048
+
+
+def _clear_lanes(inner_x, group_axis, ndim_at):
+    lower, n_now, state_next = (
+        jax.lax.axis_size(group_axis),
+        jax.lax.axis_index(group_axis),
+        inner_x.shape[ndim_at],
+    )
+    windows = list(map(lambda dev_i: (dev_i, (dev_i + 1) % lower), range(lower)))
+    by_rank = list(map(lambda dev_i: (dev_i, (dev_i - 1) % lower), range(lower)))
+    fresh = jnp.zeros(
+        (*inner_x.shape[:ndim_at], lower * state_next, *inner_x.shape[ndim_at + 1 :]), inner_x.dtype
+    )
+    v_next = all_rows = inner_x
+    left_arr = lower // 2
+    fresh = lax.dynamic_update_slice_in_dim(fresh, inner_x, n_now * state_next, axis=ndim_at)
+    for c in range(1, left_arr + 1):
+        v_next = jax.lax.ppermute(v_next, group_axis, windows)
+        fresh = lax.dynamic_update_slice_in_dim(
+            fresh, v_next, (n_now - c) % lower * state_next, axis=ndim_at
+        )
+        if c < lower - left_arr:
+            all_rows = jax.lax.ppermute(all_rows, group_axis, by_rank)
+            fresh = lax.dynamic_update_slice_in_dim(
+                fresh, all_rows, (n_now + c) % lower * state_next, axis=ndim_at
+            )
+    return fresh
 
 
 def passed_along(block, axis, distance):
@@ -160,7 +187,7 @@
     first_place = lax.axis_index("sp") * row_count
     places = first_place + jnp.arange(row_count)
     last_place = first_place + row_count - 1
-    piece_wide = lax.all_gather(tokens, "tp", axis=1, tiled=True).astype(jnp.float32)
+    piece_wide = _clear_lanes(tokens, "tp", 1).astype(jnp.float32)
     piece_low = (piece_wide * pre_gain).astype(jnp.bfloat16)
 
     def accumulate(source, weight):

time: 220 us -> 216 us (0.982)
  waiting for transfers between devices: 93.3 us -> 72.2 us
  starting transfers between devices: 21.3 us -> 28.9 us
  local copies, waits for them, and re-layouts: 22.8 us -> 30.3 us
  matrix products: 28.8 us -> 31.2 us
    all_gather x1 -> x0, waiting for transfers between devices: 30.1 us -> none  [shards(): lax.all_gather(tokens, 'tp', axis=1, tiled=True).astype(jnp.float32)]
    ppermute x0 -> x7, waiting for transfers between devices: none -> 12.4 us  [the longest x4 11.1 us: _clear_lanes(): v_next = jax.lax.ppermute(v_next, group_axis, windows)]
    ppermute x0 -> x7, starting transfers between devices: none -> 9.01 us  [the longest x3 9 us: _clear_lanes(): all_rows = jax.lax.ppermute(all_rows, group_axis, by_rank)]
    dynamic_update_slice x0 -> x8, local copies, waits for them, and re-layouts: none -> 5.98 us  [the longest x4 3.01 us: _clear_lanes(): lax.dynamic_update_slice_in_dim(fresh, v_next, (n_now - c) % lower * stat...]
    dot_general x5, matrix products: 10.7 us -> 13.1 us  [accumulate(): return jnp.dot(source, weight, preferred_element_type=jnp.float32)]
  transfers between devices with their start and end apart: 6 -> 12, of which waited for: 6 -> 10; matrix products, arithmetic and copies ran while one was open for 6% -> 10% of each run, Pallas kernels for 0% -> 0%
where the time goes in v1:
time: 216 us; the launch traced here: 215 us
  waiting for transfers between devices  72.2 us (33%)
  matrix products  31.2 us (14%)
  blocking collectives  30.5 us (14%)
  local copies, waits for them, and re-layouts  30.3 us (14%)
  starting transfers between devices  28.9 us (13%)
  between operations  14.4 us (7%)
  other arithmetic  6.98 us (3%)
    all_gather x1, waiting for transfers between devices, in_one_piece(): out = lax.all_gather(both, axis, axis=dim, tiled=True)  48.2 us
    all_to_all x1, blocking collectives, sum_at_owner(): lax.all_to_all(in_blocks(shard, dim, count), axis, 0, 0, tiled=True)  30.5 us
    all_to_all x3, starting transfers between devices, from_everyone(): return lax.all_to_all(copies, axis, split_axis=0, concat_axis=0, tiled=True)  16.8 us
    dot_general x5, matrix products, accumulate(): return jnp.dot(source, weight, preferred_element_type=jnp.float32)  13.1 us
    all_to_all x3, waiting for transfers between devices, from_everyone(): return lax.all_to_all(copies, axis, split_axis=0, concat_axis=0, tiled=True)  11.6 us
    ppermute x4, waiting for transfers between devices, _clear_lanes(): v_next = jax.lax.ppermute(v_next, group_axis, windows)  11.1 us
    ppermute x3, starting transfers between devices, _clear_lanes(): all_rows = jax.lax.ppermute(all_rows, group_axis, by_rank)  9 us
    unnamed x35, local copies, waits for them, and re-layouts  8.59 us
  transfers between devices with their start and end apart: 12, of which 10 were waited for; matrix products, arithmetic and copies ran while one was open for 10% of the time, Pallas kernels for 0%

profile of v1, /device:TPU:228, one launch (start us, length us, event | category | flops | bytes accessed | tf_op | source)
XLA Modules:
  0.0 215.0 jit_solution(17320278730199273256)
XLA Ops:
  6.6 2.9 %collective-permute-start.1 = (bf16[256,512]{1,0:T(8,128)(2,1)}, bf16[256,512]{1,0:T(8,128)(2,1)S(1)}, u32[]{:S(2)}, u32[]{:S(2)}) collective-permute-start(bf16[256,512]{1,0:T(8,128)(2,1)} %param.23), channel_id=1, source_target_pairs={{0,7},{1,0},{2,1},{3,2},{4,3},{5,4},{6,5},{7,6},{8,15},{9,8},{10,9... | collective-permute-start | bytes 786440 | tf_op jit(solution)/shard_map/ppermute | solution.py:36
  9.5 4.3 %collective-permute-done = bf16[256,512]{1,0:T(8,128)(2,1)S(1)} collective-permute-done((bf16[256,512]{1,0:T(8,128)(2,1)}, bf16[256,512]{1,0:T(8,128)(2,1)S(1)}, u32[]{:S(2)}, u32[]{:S(2)}) %collective-permute-start) | collective-permute-done | bytes 262176 | tf_op jit(solution)/shard_map/ppermute | solution.py:31
  13.8 1.5 broadcast_in_dim.43
  16.1 2.9 %collective-permute-start.3 = (bf16[256,512]{1,0:T(8,128)(2,1)S(1)}, bf16[256,512]{1,0:T(8,128)(2,1)S(1)}, u32[]{:S(2)}, u32[]{:S(2)}) collective-permute-start(bf16[256,512]{1,0:T(8,128)(2,1)S(1)} %collective-permute-done.1), channel_id=1, source_target_pairs={{0,7},{1,0},{2,1},{3,2},{4,3},{5,4},{6,5},{7,6},{8,15},{9,8},{10,9... | collective-permute-start | bytes 786440 | tf_op jit(solution)/shard_map/ppermute | solution.py:36
  19.0 1.7 collective-permute-done.2
  22.9 3.1 %collective-permute-start.5 = (bf16[256,512]{1,0:T(8,128)(2,1)S(1)}, bf16[256,512]{1,0:T(8,128)(2,1)S(1)}, u32[]{:S(2)}, u32[]{:S(2)}) collective-permute-start(bf16[256,512]{1,0:T(8,128)(2,1)S(1)} %collective-permute-done.3), channel_id=1, source_target_pairs={{0,7},{1,0},{2,1},{3,2},{4,3},{5,4},{6,5},{7,6},{8,15},{9,8},{10,9... | collective-permute-start | bytes 786440 | tf_op jit(solution)/shard_map/ppermute | solution.py:36
  30.6 4.2 %collective-permute-done.6 = bf16[256,512]{1,0:T(8,128)(2,1)S(1)} collective-permute-done((bf16[256,512]{1,0:T(8,128)(2,1)S(1)}, bf16[256,512]{1,0:T(8,128)(2,1)S(1)}, u32[]{:S(2)}, u32[]{:S(2)}) %collective-permute-start.6) | collective-permute-done | bytes 262176 | tf_op jit(solution)/shard_map/ppermute | solution.py:31
  35.5 2.2 %fusion.16 = f32[256]{0:T(256)S(1)} fusion(bf16[256,4096]{1,0:T(8,128)(2,1)} %constant_dynamic-update-slice_fusion), kind=kLoop, calls=%fused_computation.29 | loop fusion | flops 3145472 | bytes 2098176 | tf_op jit(solution)/shard_map/reduce_sum | solution.py:196
  37.8 2.4 %convolution_multiply_fusion.4 = f32[256,64]{0,1:T(8,128)S(1)} fusion(bf16[4096,64]{0,1:T(8,128)(2,1)S(1)} %copy-done.11, bf16[256,4096]{1,0:T(8,128)(2,1)} %constant_dynamic-update-slice_fusion, f32[4096]{0:T(1024)S(1)} %copy-done.14, f32[256]{0:T(256)S(1)} %add_rsqrt_fusion.3), kind=kOutput, calls=%fused_computation.51 | convolution fusion | flops 137379840 | bytes 2704384 | tf_op jit(solution)/shard_map/dot_general | solution.py:194
  40.2 3.1 %multiply_reduce_fusion.1 = (f32[256]{0:T(256)S(1)}, f32[256,512]{1,0:T(8,128)S(1)}) fusion(bf16[4096,512]{1,0:T(8,128)(2,1)S(1)} %copy-done.10, bf16[256,4096]{1,0:T(8,128)(2,1)} %constant_dynamic-update-slice_fusion, f32[4096]{0:T(1024)S(1)} %copy-done.14, f32[256]{0:T(256)S(1)} %add_rsqrt_fusion.3), kind=kOutput, calls=%fused_computation.55 | convolution fusion | flops 1077280512 | bytes 6834176 | tf_op jit(solution)/shard_map/dot_general | solution.py:194
  44.6 2.6 %fusion.29 = bf16[256,128]{1,0:T(8,128)(2,1)S(1)} fusion(bf16[4096,128]{1,0:T(8,128)(2,1)} %param.26, bf16[256,4096]{1,0:T(8,128)(2,1)} %constant_dynamic-update-slice_fusion, f32[4096]{0:T(1024)S(1)} %copy-done.14, f32[256]{0:T(256)S(1)} %add_rsqrt_fusion.3), kind=kOutput, calls=%fused_computation.50 | convolution fusion | flops 271646720 | bytes 3228672 | tf_op jit(solution)/shard_map/dot_general | solution.py:194
  47.2 3.1 %collective-permute-start.7 = (bf16[3,128]{1,0:T(4,128)(2,1)S(1)}, bf16[3,128]{1,0:T(4,128)(2,1)S(1)}, u32[]{:S(2)}, u32[]{:S(2)}) collective-permute-start(bf16[3,128]{1,0:T(4,128)(2,1)S(1)} %slice.463), channel_id=1, source_target_pairs={{0,8},{8,16},{16,24},{24,32},{32,40},{40,48},{48,56},{56,64},{64,7... | collective-permute-start | bytes 2312 | tf_op jit(solution)/shard_map/ppermute | solution.py:46
  50.4 2.5 %fusion.18 = f32[256,1,192]{0,2,1:T(8,128)S(1)} fusion(bf16[4096,192]{0,1:T(8,128)(2,1)S(1)} %copy-done, bf16[256,4096]{1,0:T(8,128)(2,1)} %constant_dynamic-update-slice_fusion, f32[4096]{0:T(1024)S(1)} %copy-done.14, f32[256]{0:T(256)S(1)} %add_rsqrt_fusion.3), kind=kOutput, calls=%fused_computation.35 | convolution fusion | flops 405848064 | bytes 3884032 | tf_op jit(solution)/shard_map/dot_general | solution.py:194
  55.9 9.2 %all-to-all-start = ((f32[32,2,128]{2,1,0:T(2,128)}), f32[32,2,128]{2,1,0:T(2,128)S(1)}, u32[]{:S(2)}, u32[]{:S(2)}) async-start(f32[32,2,128]{2,1,0:T(2,128)} %broadcast_in_dim.45), calls=%async_computation | async-start | bytes 65536 | tf_op jit(solution)/shard_map/all_to_all | solution.py:51
  65.3 5.3 %all-to-all-done = f32[32,2,128]{2,1,0:T(2,128)S(1)} async-done(((f32[32,2,128]{2,1,0:T(2,128)}), f32[32,2,128]{2,1,0:T(2,128)S(1)}, u32[]{:S(2)}, u32[]{:S(2)}) %all-to-all-start) | async-done | bytes 32800 | tf_op jit(solution)/shard_map/all_to_all | solution.py:51
  71.0 2.7 %multiply_reduce_fusion.2 = (f32[256]{0:T(256)S(1)}, f32[256,128]{1,0:T(8,128)S(1)}) fusion(bf16[4096,128]{1,0:T(8,128)(2,1)} %param.27, bf16[256,4096]{1,0:T(8,128)(2,1)} %constant_dynamic-update-slice_fusion, f32[4096]{0:T(1024)S(1)} %copy-done.14, f32[256]{0:T(256)S(1)} %add_rsqrt_fusion.3, f32[128]{0:T(128)S(1)} %add_bitcast_fusion, ...), kind=kOutput, calls=%fused_computation.75 | convolution fusion | flops 272105216 | bytes 3820032 | tf_op jit(solution)/shard_map/dot_general | solution.py:194
  74.3 3.3 %all-to-all-start.1 = ((f32[8,256,1]{1,2,0:T(1,128)}), f32[8,256,1]{1,2,0:T(1,128)S(1)}, u32[]{:S(2)}, u32[]{:S(2)}) async-start(f32[8,256,1]{1,2,0:T(1,128)} %broadcast_in_dim.73), calls=%async_computation.1 | async-start | bytes 16384 | tf_op jit(solution)/shard_map/all_to_all | solution.py:51
  77.7 5.1 %all-to-all-done.1 = f32[8,256,1]{1,2,0:T(1,128)S(1)} async-done(((f32[8,256,1]{1,2,0:T(1,128)}), f32[8,256,1]{1,2,0:T(1,128)S(1)}, u32[]{:S(2)}, u32[]{:S(2)}) %all-to-all-start.1) | async-done | bytes 8224 | tf_op jit(solution)/shard_map/all_to_all | solution.py:51
  82.8 48.2 %all-gather.2.cloned.1.call-done = bf16[8192,320]{0,1:T(8,128)(2,1)} async-done(((bf16[256,320]{0,1:T(8,128)(2,1)}), bf16[8192,320]{0,1:T(8,128)(2,1)}) %all-gather.2.cloned.1.call-update) | async-done | bytes 5242896 | tf_op jit(solution)/shard_map/all_gather | solution.py:100
  131.0 4.7 %split.8 = bf16[8192,256]{0,1:T(8,128)(2,1)} slice(bf16[8192,320]{0,1:T(8,128)(2,1)} %all-gather.2.cloned.1.call-done), slice={[0:8192], [0:256]} | slice | bytes 8388608 | tf_op jit(solution)/shard_map/split | solution.py:101
  135.7 6.4 %copy.31 = bf16[8192,256]{1,0:T(8,128)(2,1)} copy(bf16[8192,256]{0,1:T(8,128)(2,1)} %split.8) | data formatting | bytes 8388608
  143.3 1.8 copy.33
  145.1 17.6 %while.18 = (s32[]{:T(128)}, f32[1,256]{1,0:T(1,128)S(1)}, f32[1,256]{1,0:T(1,128)S(1)}, f32[1,256,128]{2,1,0:T(8,128)S(1)}, s32[]{:T(128)}, /*index=5*/bf16[819...) while((s32[]{:T(128)}, f32[1,256]{1,0:T(1,128)S(1)}, ...), condition=%wide.region_9.10_spmd.clone, body=%wide.region_4.9_spmd.clone.sunk | while | flops 340332288 | bytes 14554469 | solution.py:281
  145.1 4.4 %conditional.3 = ((f32[1,256]{1,0:T(1,128)S(1)}, f32[1,256]{1,0:T(1,128)S(1)}, f32[1,256,128]{2,1,0:T(8,128)S(1)})) conditional(s32[]{:T(128)} %convert_element_type.205, (f32[1,256]{1,0:T(1,128)S(1)}, f32[1,256]{1,0:T(1,128)S(1)}, f32[1,256,128]{2,1,0:T(8,128)S(1)}) %tuple.82, (s32[]{:T(128)}, s32[]{:T(128)}, s32[]{:T(128)}, ...), branch_computations={%region_5.5_spmd, %region_6.8_spmd} | conditional | flops 340332288 | bytes 14553182 | solution.py:279
  146.5 1.5 convolution_bitcast_fusion
  149.5 4.3 %conditional.3 = ((f32[1,256]{1,0:T(1,128)S(1)}, f32[1,256]{1,0:T(1,128)S(1)}, f32[1,256,128]{2,1,0:T(8,128)S(1)})) conditional(s32[]{:T(128)} %convert_element_type.205, (f32[1,256]{1,0:T(1,128)S(1)}, f32[1,256]{1,0:T(1,128)S(1)}, f32[1,256,128]{2,1,0:T(8,128)S(1)}) %tuple.82, (s32[]{:T(128)}, s32[]{:T(128)}, s32[]{:T(128)}, ...), branch_computations={%region_5.5_spmd, %region_6.8_spmd} | conditional | flops 340332288 | bytes 14553182 | solution.py:279
  153.9 4.4 %conditional.3 = ((f32[1,256]{1,0:T(1,128)S(1)}, f32[1,256]{1,0:T(1,128)S(1)}, f32[1,256,128]{2,1,0:T(8,128)S(1)})) conditional(s32[]{:T(128)} %convert_element_type.205, (f32[1,256]{1,0:T(1,128)S(1)}, f32[1,256]{1,0:T(1,128)S(1)}, f32[1,256,128]{2,1,0:T(8,128)S(1)}) %tuple.82, (s32[]{:T(128)}, s32[]{:T(128)}, s32[]{:T(128)}, ...), branch_computations={%region_5.5_spmd, %region_6.8_spmd} | conditional | flops 340332288 | bytes 14553182 | solution.py:279
  158.3 4.3 %conditional.3 = ((f32[1,256]{1,0:T(1,128)S(1)}, f32[1,256]{1,0:T(1,128)S(1)}, f32[1,256,128]{2,1,0:T(8,128)S(1)})) conditional(s32[]{:T(128)} %convert_element_type.205, (f32[1,256]{1,0:T(1,128)S(1)}, f32[1,256]{1,0:T(1,128)S(1)}, f32[1,256,128]{2,1,0:T(8,128)S(1)}) %tuple.82, (s32[]{:T(128)}, s32[]{:T(128)}, s32[]{:T(128)}, ...), branch_computations={%region_5.5_spmd, %region_6.8_spmd} | conditional | flops 340332288 | bytes 14553182 | solution.py:279
  163.5 4.3 %all-to-all-start.2 = ((f32[8,256,1]{1,2,0:T(1,128)}), f32[8,256,1]{1,2,0:T(1,128)S(1)}, u32[]{:S(2)}, u32[]{:S(2)}) async-start(f32[8,256,1]{1,2,0:T(1,128)} %broadcast_in_dim.76), calls=%async_computation.2 | async-start | bytes 16384 | tf_op jit(solution)/shard_map/all_to_all | solution.py:51
  167.8 4.0 %fusion.54 = f32[256,4096]{1,0:T(8,128)} fusion(bf16[128,4096]{1,0:T(8,128)(2,1)} %param.39, f32[256,128]{1,0:T(8,128)S(1)} %get-tuple-element.364, f32[128]{0:T(128)S(1)} %copy-done.6, f32[256]{0:T(256)S(1)} %add_rsqrt_fusion.2), kind=kOutput, calls=%fused_computation.81 | convolution fusion | flops 268533760 | bytes 5375488 | tf_op jit(solution)/shard_map/dot_general | solution.py:295
  173.1 3.0 %fusion.15 = bf16[256,4096]{1,0:T(8,128)(2,1)S(1)} fusion(f32[256,4096]{1,0:T(8,128)} %fusion.54, bf16[128,4096]{1,0:T(8,128)(2,1)S(1)} %copy-done.1, f32[128]{0:T(128)S(1)} %copy-done.9, f32[256]{0:T(256)S(1)} %add_rsqrt_fusion, f32[1,256,128]{2,1,0:T(8,128)S(1)} %get-tuple-element.220, f32[256]{0:T(256)S(1)} %bitcast.96), kind=kOutput, calls=%fused_computation.28 | convolution fusion | flops 270663680 | bytes 7473664 | tf_op jit(solution)/shard_map/dot_general | solution.py:296
  176.1 30.5 %all_to_all.20 = bf16[8,32,4096]{2,1,0:T(8,128)(2,1)S(1)} all-to-all(bf16[8,32,4096]{2,1,0:T(8,128)(2,1)S(1)} %bitcast.87), channel_id=1, replica_groups=mesh['sp'=32,'tp'=8] {'tp'}, dimensions={0} | all-to-all | bytes 4194304 | tf_op jit(solution)/shard_map/all_to_all | solution.py:111
  (278 shorter events, 33.9 us)
Async XLA Ops:
  6.5 43.8 %copy-start = (bf16[4096,192]{0,1:T(8,128)(2,1)S(1)}, bf16[4096,192]{0,1:T(8,128)(2,1)}, u32[]{:S(2)}) copy-start(bf16[4096,192]{0,1:T(8,128)(2,1)} %param.32) | copy-start | bytes 4718596
  6.5 8.8 %copy-start.2 = (bf16[256,512]{1,0:T(8,128)(2,1)S(1)}, bf16[256,512]{1,0:T(8,128)(2,1)}, u32[]{:S(2)}) copy-start(bf16[256,512]{1,0:T(8,128)(2,1)} %param.23) | copy-start | bytes 786436
  6.5 124.5 %all-gather.2.cloned.1.call-start = ((), (), s32[]{:S(2)}) async-start(), calls=%async_computation.4 | async-start | bytes 5406720 | tf_op jit(solution)/shard_map/all_gather | solution.py:100
  6.5 7.2 %collective-permute-start = (bf16[256,512]{1,0:T(8,128)(2,1)}, bf16[256,512]{1,0:T(8,128)(2,1)S(1)}, u32[]{:S(2)}, u32[]{:S(2)}) collective-permute-start(bf16[256,512]{1,0:T(8,128)(2,1)} %param.23), channel_id=1, source_target_pairs={{0,1},{1,2},{2,3},{3,4},{4,5},{5,6},{6,7},{7,0},{8,9},{9,10},{10,1... | collective-permute-start | bytes 786440 | tf_op jit(solution)/shard_map/ppermute | solution.py:31
  6.6 9.5 %collective-permute-start.1 = (bf16[256,512]{1,0:T(8,128)(2,1)}, bf16[256,512]{1,0:T(8,128)(2,1)S(1)}, u32[]{:S(2)}, u32[]{:S(2)}) collective-permute-start(bf16[256,512]{1,0:T(8,128)(2,1)} %param.23), channel_id=1, source_target_pairs={{0,7},{1,0},{2,1},{3,2},{4,3},{5,4},{6,5},{7,6},{8,15},{9,8},{10,9... | collective-permute-start | bytes 786440 | tf_op jit(solution)/shard_map/ppermute | solution.py:36
  13.8 7.0 %collective-permute-start.2 = (bf16[256,512]{1,0:T(8,128)(2,1)S(1)}, bf16[256,512]{1,0:T(8,128)(2,1)S(1)}, u32[]{:S(2)}, u32[]{:S(2)}) collective-permute-start(bf16[256,512]{1,0:T(8,128)(2,1)S(1)} %collective-permute-done), channel_id=1, source_target_pairs={{0,1},{1,2},{2,3},{3,4},{4,5},{5,6},{6,7},{7,0},{8,9},{9,10},{10,1... | collective-permute-start | bytes 786440 | tf_op jit(solution)/shard_map/ppermute | solution.py:31
  16.1 6.8 %collective-permute-start.3 = (bf16[256,512]{1,0:T(8,128)(2,1)S(1)}, bf16[256,512]{1,0:T(8,128)(2,1)S(1)}, u32[]{:S(2)}, u32[]{:S(2)}) collective-permute-start(bf16[256,512]{1,0:T(8,128)(2,1)S(1)} %collective-permute-done.1), channel_id=1, source_target_pairs={{0,7},{1,0},{2,1},{3,2},{4,3},{5,4},{6,5},{7,6},{8,15},{9,8},{10,9... | collective-permute-start | bytes 786440 | tf_op jit(solution)/shard_map/ppermute | solution.py:36
  20.8 7.0 %collective-permute-start.4 = (bf16[256,512]{1,0:T(8,128)(2,1)S(1)}, bf16[256,512]{1,0:T(8,128)(2,1)S(1)}, u32[]{:S(2)}, u32[]{:S(2)}) collective-permute-start(bf16[256,512]{1,0:T(8,128)(2,1)S(1)} %collective-permute-done.2), channel_id=1, source_target_pairs={{0,1},{1,2},{2,3},{3,4},{4,5},{5,6},{6,7},{7,0},{8,9},{9,10},{10,1... | collective-permute-start | bytes 786440 | tf_op jit(solution)/shard_map/ppermute | solution.py:31
  22.9 7.0 %collective-permute-start.5 = (bf16[256,512]{1,0:T(8,128)(2,1)S(1)}, bf16[256,512]{1,0:T(8,128)(2,1)S(1)}, u32[]{:S(2)}, u32[]{:S(2)}) collective-permute-start(bf16[256,512]{1,0:T(8,128)(2,1)S(1)} %collective-permute-done.3), channel_id=1, source_target_pairs={{0,7},{1,0},{2,1},{3,2},{4,3},{5,4},{6,5},{7,6},{8,15},{9,8},{10,9... | collective-permute-start | bytes 786440 | tf_op jit(solution)/shard_map/ppermute | solution.py:36
  26.8 11.0 %copy-start.11 = (bf16[4096,64]{0,1:T(8,128)(2,1)S(1)}, bf16[4096,64]{0,1:T(8,128)(2,1)}, u32[]{:S(2)}) copy-start(bf16[4096,64]{0,1:T(8,128)(2,1)} %param.34) | copy-start | bytes 1572868
  26.8 11.0 %copy-start.14 = (f32[4096]{0:T(1024)S(1)}, f32[4096]{0:T(1024)}, u32[]{:S(2)}) copy-start(f32[4096]{0:T(1024)} %param.24) | copy-start | bytes 49156
  27.8 7.0 %collective-permute-start.6 = (bf16[256,512]{1,0:T(8,128)(2,1)S(1)}, bf16[256,512]{1,0:T(8,128)(2,1)S(1)}, u32[]{:S(2)}, u32[]{:S(2)}) collective-permute-start(bf16[256,512]{1,0:T(8,128)(2,1)S(1)} %collective-permute-done.4), channel_id=1, source_target_pairs={{0,1},{1,2},{2,3},{3,4},{4,5},{5,6},{6,7},{7,0},{8,9},{9,10},{10,1... | collective-permute-start | bytes 786440 | tf_op jit(solution)/shard_map/ppermute | solution.py:31
  35.5 4.6 %copy-start.10 = (bf16[4096,512]{1,0:T(8,128)(2,1)S(1)}, bf16[4096,512]{1,0:T(8,128)(2,1)}, u32[]{:S(2)}) copy-start(bf16[4096,512]{1,0:T(8,128)(2,1)} %param.33) | copy-start | bytes 12582916
  40.2 3.3 %copy-start.3 = (bf16[512,256]{1,0:T(8,128)(2,1)S(1)}, bf16[512,256]{1,0:T(8,128)(2,1)}, u32[]{:S(2)}) copy-start(bf16[512,256]{1,0:T(8,128)(2,1)} %param.36) | copy-start | bytes 786436
  40.2 3.3 %copy-start.5 = (f32[512]{0:T(512)S(1)}, f32[512]{0:T(512)}, u32[]{:S(2)}) copy-start(f32[512]{0:T(512)} %param.35) | copy-start | bytes 6148
  40.2 4.4 %copy-start.15 = (f32[128]{0:T(128)S(1)}, f32[128]{0:T(128)}, u32[]{:S(2)}) copy-start(f32[128]{0:T(128)} %param.31) | copy-start | bytes 1540
  40.2 4.4 %copy-start.8 = (f32[256]{0:T(256)S(1)}, f32[256]{0:T(256)}, u32[]{:S(2)}) copy-start(f32[256]{0:T(256)} %param.25) | copy-start | bytes 3076
  40.2 4.4 %copy-start.7 = (f32[4,128]{1,0:T(4,128)S(1)}, f32[4,128]{1,0:T(4,128)}, u32[]{:S(2)}) copy-start(f32[4,128]{1,0:T(4,128)} %param.28) | copy-start | bytes 6148
  47.2 5.6 %copy-start.12 = (bf16[1,128,128]{2,1,0:T(8,128)(2,1)S(1)}, bf16[1,128,128]{2,1,0:T(8,128)(2,1)}, u32[]{:S(2)}) copy-start(bf16[1,128,128]{2,1,0:T(8,128)(2,1)} %param.29) | copy-start | bytes 98308
  47.2 5.8 %copy-start.13 = (bf16[1,128,128]{2,1,0:T(8,128)(2,1)S(1)}, bf16[1,128,128]{2,1,0:T(8,128)(2,1)}, u32[]{:S(2)}) copy-start(bf16[1,128,128]{2,1,0:T(8,128)(2,1)} %param.30) | copy-start | bytes 98308
  47.2 5.6 %collective-permute-start.7 = (bf16[3,128]{1,0:T(4,128)(2,1)S(1)}, bf16[3,128]{1,0:T(4,128)(2,1)S(1)}, u32[]{:S(2)}, u32[]{:S(2)}) collective-permute-start(bf16[3,128]{1,0:T(4,128)(2,1)S(1)} %slice.463), channel_id=1, source_target_pairs={{0,8},{8,16},{16,24},{24,32},{32,40},{40,48},{48,56},{56,64},{64,7... | collective-permute-start | bytes 2312 | tf_op jit(solution)/shard_map/ppermute | solution.py:46
  55.9 14.7 %all-to-all-start = ((f32[32,2,128]{2,1,0:T(2,128)}), f32[32,2,128]{2,1,0:T(2,128)S(1)}, u32[]{:S(2)}, u32[]{:S(2)}) async-start(f32[32,2,128]{2,1,0:T(2,128)} %broadcast_in_dim.45), calls=%async_computation | async-start | bytes 65536 | tf_op jit(solution)/shard_map/all_to_all | solution.py:51
  74.3 8.5 %all-to-all-start.1 = ((f32[8,256,1]{1,2,0:T(1,128)}), f32[8,256,1]{1,2,0:T(1,128)S(1)}, u32[]{:S(2)}, u32[]{:S(2)}) async-start(f32[8,256,1]{1,2,0:T(1,128)} %broadcast_in_dim.73), calls=%async_computation.1 | async-start | bytes 16384 | tf_op jit(solution)/shard_map/all_to_all | solution.py:51
  142.1 1.2 slice-start
  145.1 22.7 %copy-start.6 = (f32[128]{0:T(128)S(1)}, f32[128]{0:T(128)}, u32[]{:S(2)}) copy-start(f32[128]{0:T(128)} %param.37) | copy-start | bytes 1540
  163.5 9.6 %all-to-all-start.2 = ((f32[8,256,1]{1,2,0:T(1,128)}), f32[8,256,1]{1,2,0:T(1,128)S(1)}, u32[]{:S(2)}, u32[]{:S(2)}) async-start(f32[8,256,1]{1,2,0:T(1,128)} %broadcast_in_dim.76), calls=%async_computation.2 | async-start | bytes 16384 | tf_op jit(solution)/shard_map/all_to_all | solution.py:51
  167.8 5.3 %copy-start.1 = (bf16[128,4096]{1,0:T(8,128)(2,1)S(1)}, bf16[128,4096]{1,0:T(8,128)(2,1)}, u32[]{:S(2)}) copy-start(bf16[128,4096]{1,0:T(8,128)(2,1)} %param.40) | copy-start | bytes 3145732
  167.8 5.3 %copy-start.9 = (f32[128]{0:T(128)S(1)}, f32[128]{0:T(128)}, u32[]{:S(2)}) copy-start(f32[128]{0:T(128)} %param.38) | copy-start | bytes 1540
  206.7 0.7 copy-start.4
Sparse Core Ops, SparseCore 0:
  44.7 86.2 all-gather.1
